TPU v7x, 32 devices: a whole 2x2x4 slice. The times are simulated.
32 devices in a mesh: rep: 2 (over x), fs: 8 (over z, y), tp: 2 (over core).
Axes of the slice: x: 2, y: 2, z: 4, core: 2. Of those that a mesh axis runs over, the one named last changes fastest.
Arguments:
- tokens: bfloat16 [8192, 2048], P(('rep', 'fs')), may hold values from -6 to 6
- mix_gain: bfloat16 [2048], replicated, may hold values from 0.099609375 to 1.8984375
- value_weight: bfloat16 [2048, 1536], P('fs', 'tp'), may hold values from -0.125 to 0.125
- outer_gate_weight: bfloat16 [2048, 1536], P('fs', 'tp'), may hold values from -0.125 to 0.125
- inner_gate_weight: bfloat16 [2048, 1536], P('fs', 'tp'), may hold values from -0.125 to 0.125
- conv_taps: bfloat16 [3, 1536], P(None, 'tp'), may hold values from -3 to 3
- mix_out_weight: bfloat16 [1536, 2048], P('tp', 'fs'), may hold values from -0.15625 to 0.15625
- ffn_gain: bfloat16 [2048], replicated, may hold values from 0.099609375 to 1.8984375
- gate_weight: bfloat16 [2048, 4096], P('fs', 'tp'), may hold values from -0.125 to 0.125
- up_weight: bfloat16 [2048, 4096], P('fs', 'tp'), may hold values from -0.125 to 0.125
- down_weight: bfloat16 [4096, 2048], P('tp', 'fs'), may hold values from -0.09375 to 0.09375
Outputs:
- layer_out: bfloat16 [8192, 2048], P(('rep', 'fs'))
All inputs are finite; a program needn't handle non-finite values.
Results may differ from a plain program's by a relative error of at most 0.02.
Values may be sent and summed in bfloat16 or wider, within the bound.
A program may use at most 128 MiB of HBM per device.

v0:
```python
import jax
import jax.numpy as jnp
from jax import lax
from jax.sharding import PartitionSpec as P

SEQ_GRP = 2
EPS = 1e-05


def rms_norm(values, gain):
    floats = values.astype(jnp.float32)
    scaled = floats * lax.rsqrt(jnp.mean(floats * floats, axis=-1, keepdims=True) + EPS)
    return (scaled * gain.astype(jnp.float32)).astype(jnp.bfloat16)


def short_conv(value_proj, outer_proj, inner_proj, conv_taps, seq_len):
    mixed_in = inner_proj.astype(jnp.float32) * value_proj.astype(jnp.float32)
    count_rows = mixed_in.shape[0]
    position = (jnp.arange(count_rows, dtype=jnp.int32) % seq_len)[:, None]
    zero_row = jnp.zeros((1, mixed_in.shape[1]), jnp.float32)
    back_one = jnp.where(position >= 1, jnp.concatenate([zero_row, mixed_in[:-1]], axis=0), 0.0)
    back_two = jnp.where(
        position >= 2, jnp.concatenate([zero_row, zero_row, mixed_in[:-2]], axis=0), 0.0
    )
    taps = conv_taps.astype(jnp.float32)
    convolved = taps[0] * back_two + taps[1] * back_one + taps[2] * mixed_in
    return (outer_proj.astype(jnp.float32) * convolved).astype(jnp.bfloat16)


def local(
    tokens,
    mix_gain,
    value_weight,
    outer_gate_weight,
    inner_gate_weight,
    conv_taps,
    mix_out_weight,
    ffn_gain,
    gate_weight,
    up_weight,
    down_weight,
):
    row_count = tokens.shape[0]
    share = row_count // lax.axis_size("tp")
    seq_len = row_count // SEQ_GRP
    own_rows = lax.dynamic_slice_in_dim(tokens, lax.axis_index("tp") * share, share, 0).astype(
        jnp.float32
    )
    normed = rms_norm(tokens, mix_gain)
    value_full, outer_full, inner_full, mix_out_full, gate_full, up_full, down_full = (
        lax.all_gather(value_weight, "fs", axis=0, tiled=True),
        lax.all_gather(outer_gate_weight, "fs", axis=0, tiled=True),
        lax.all_gather(inner_gate_weight, "fs", axis=0, tiled=True),
        lax.all_gather(mix_out_weight, "fs", axis=1, tiled=True),
        lax.all_gather(gate_weight, "fs", axis=0, tiled=True),
        lax.all_gather(up_weight, "fs", axis=0, tiled=True),
        lax.all_gather(down_weight, "fs", axis=1, tiled=True),
    )
    value_proj = jnp.dot(normed, value_full, preferred_element_type=jnp.float32).astype(
        jnp.bfloat16
    )
    outer_proj = jnp.dot(normed, outer_full, preferred_element_type=jnp.float32).astype(
        jnp.bfloat16
    )
    inner_proj = jnp.dot(normed, inner_full, preferred_element_type=jnp.float32).astype(
        jnp.bfloat16
    )
    mixed = short_conv(value_proj, outer_proj, inner_proj, conv_taps, seq_len)
    picked = mixed
    mix_total = lax.psum_scatter(
        jnp.dot(picked, mix_out_full, preferred_element_type=jnp.float32).astype(jnp.bfloat16),
        "tp",
        scatter_dimension=0,
        tiled=True,
    ).astype(jnp.float32)
    after_mix = (own_rows + mix_total).astype(jnp.bfloat16)
    normed_two = rms_norm(after_mix, ffn_gain)
    block_rows = lax.all_gather(normed_two, "tp", axis=0, tiled=True)
    gate_proj = jnp.dot(block_rows, gate_full, preferred_element_type=jnp.float32)
    up_proj = jnp.dot(block_rows, up_full, preferred_element_type=jnp.float32)
    hidden = (jax.nn.silu(gate_proj) * up_proj).astype(jnp.bfloat16)
    picked = hidden
    ffn_total = lax.psum_scatter(
        jnp.dot(picked, down_full, preferred_element_type=jnp.float32).astype(jnp.bfloat16),
        "tp",
        scatter_dimension=0,
        tiled=True,
    ).astype(jnp.float32)
    finished = (after_mix.astype(jnp.float32) + ffn_total).astype(jnp.bfloat16)
    return lax.all_gather(finished, "tp", axis=0, tiled=True)


def solution(mesh):
    placed = (
        P(("rep", "fs"), None),
        P(),
        P("fs", "tp"),
        P("fs", "tp"),
        P("fs", "tp"),
        P(None, "tp"),
        P("tp", "fs"),
        P(),
        P("fs", "tp"),
        P("fs", "tp"),
        P("tp", "fs"),
    )
    return jax.shard_map(
        local, mesh=mesh, in_specs=placed, out_specs=P(("rep", "fs"), None), check_vma=False
    )
```

profile of v0, /device:TPU:0, one launch (start us, length us, event | category | flops | bytes accessed | tf_op | source)
XLA Modules:
  0.0 718.0 jit_solution(16249208888733937228)
XLA Ops:
  6.5 0.7 all-gather.14.cloned.1.call-update
  7.3 0.7 all-gather.12.cloned.1.call-update
  8.1 0.7 all-gather.10.cloned.1.call-update
  8.8 0.5 all-gather.16.cloned.1.call-update
  9.4 0.7 convert_element_type.69
  10.1 0.7 convert_element_type.73
  10.8 2.1 fusion
  12.9 59.4 %all-gather.14.cloned.1.call-done = bf16[2048,768]{1,0:T(8,128)(2,1)} async-done(((bf16[256,768]{1,0:T(8,128)(2,1)}), bf16[2048,768]{1,0:T(8,128)(2,1)}) %all-gather.14.cloned.1.call-update) | async-done | bytes 3145744 | tf_op jit(solution)/shard_map/all_gather | solution.py:51
  72.3 3.7 convolution_convert_fusion.2
  76.0 57.2 %all-gather.12.cloned.1.call-done = bf16[2048,768]{1,0:T(8,128)(2,1)} async-done(((bf16[256,768]{1,0:T(8,128)(2,1)}), bf16[2048,768]{1,0:T(8,128)(2,1)}) %all-gather.12.cloned.1.call-update) | async-done | bytes 3145744 | tf_op jit(solution)/shard_map/all_gather | solution.py:53
  133.2 4.9 convert_multiply_fusion.4
  138.1 56.0 %all-gather.10.cloned.1.call-done = bf16[2048,768]{1,0:T(8,128)(2,1)} async-done(((bf16[256,768]{1,0:T(8,128)(2,1)}), bf16[2048,768]{1,0:T(8,128)(2,1)}) %all-gather.10.cloned.1.call-update) | async-done | bytes 3145744 | tf_op jit(solution)/shard_map/all_gather | solution.py:52
  194.1 63.2 %all-gather.16.cloned.1.call-done = bf16[768,2048]{1,0:T(8,128)(2,1)} async-done(((bf16[768,256]{1,0:T(8,128)(2,1)}), bf16[768,2048]{1,0:T(8,128)(2,1)}) %all-gather.16.cloned.1.call-update) | async-done | bytes 3145744 | tf_op jit(solution)/shard_map/all_gather | solution.py:54
  257.3 9.8 %convolution_convert_fusion.1 = bf16[512,2048]{1,0:T(8,128)(2,1)} fusion(bf16[768,2048]{1,0:T(8,128)(2,1)} %all-gather.16.cloned.1.call-done, f32[512,768]{1,0:T(8,128)} %convert_multiply_fusion.4, f32[511,768]{1,0:T(8,128)} %bitcast.20, f32[510,768]{1,0:T(8,128)} %bitcast.21, bf16[2048,768]{1,0:T(8,128)(2,1)} %all-gather.10.cloned.1.call-done, ...), kind=kOutput, calls=%fused_computation.10 | convolution fusion | flops 3230793728 | bytes 15215616 | tf_op jit(solution)/shard_map/dot_general | solution.py:71
  267.2 0.6 copy-done.1
  267.8 7.4 %reduce-scatter.3.cloned.1.call-done = bf16[256,2048]{1,0:T(8,128)(2,1)} async-done(((bf16[512,2048]{1,0:T(8,128)(2,1)}), bf16[256,2048]{1,0:T(8,128)(2,1)}) %reduce-scatter.3.cloned.1.call-update) | async-done | bytes 1048592 | tf_op jit(solution)/shard_map/reduce_scatter | solution.py:70
  275.3 1.7 fusion.3
  277.0 1.3 fusion.5
  278.4 0.7 all-gather.20.cloned.1.call-update
  279.1 0.7 all-gather.22.cloned.1.call-update
  279.9 0.7 all-gather.24.cloned.1.call-update
  280.6 0.2 reduce-scatter.5.cloned.1.call-start
  280.8 9.6 %all-gather.18.cloned.1.call-done = bf16[512,2048]{1,0:T(8,128)(2,1)} async-done(((bf16[256,2048]{1,0:T(8,128)(2,1)}), bf16[512,2048]{1,0:T(8,128)(2,1)}) %all-gather.18.cloned.1.call-update) | async-done | bytes 2097168 | tf_op jit(solution)/shard_map/all_gather | solution.py:78
  290.4 127.8 %all-gather.20.cloned.1.call-done = bf16[2048,2048]{1,0:T(8,128)(2,1)} async-done(((bf16[256,2048]{1,0:T(8,128)(2,1)}), bf16[2048,2048]{1,0:T(8,128)(2,1)}) %all-gather.20.cloned.1.call-update) | async-done | bytes 8388624 | tf_op jit(solution)/shard_map/all_gather | solution.py:55
  418.2 10.5 %fusion.17 = f32[512,2048]{1,0:T(8,128)} fusion(bf16[512,2048]{1,0:T(8,128)(2,1)} %all-gather.18.cloned.1.call-done, bf16[2048,2048]{1,0:T(8,128)(2,1)} %all-gather.20.cloned.1.call-done), kind=kOutput, calls=%fused_computation.34 | convolution fusion | flops 4294967296 | bytes 14680064 | tf_op jit(solution)/shard_map/dot_general | solution.py:79
  428.6 114.3 %all-gather.22.cloned.1.call-done = bf16[2048,2048]{1,0:T(8,128)(2,1)} async-done(((bf16[256,2048]{1,0:T(8,128)(2,1)}), bf16[2048,2048]{1,0:T(8,128)(2,1)}) %all-gather.22.cloned.1.call-update) | async-done | bytes 8388624 | tf_op jit(solution)/shard_map/all_gather | solution.py:56
  543.0 125.2 %all-gather.24.cloned.1.call-done = bf16[2048,2048]{1,0:T(8,128)(2,1)} async-done(((bf16[2048,256]{1,0:T(8,128)(2,1)}), bf16[2048,2048]{1,0:T(8,128)(2,1)}) %all-gather.24.cloned.1.call-update) | async-done | bytes 8388624 | tf_op jit(solution)/shard_map/all_gather | solution.py:57
  668.2 17.4 %convolution_convert_fusion = bf16[512,2048]{1,0:T(8,128)(2,1)} fusion(bf16[2048,2048]{1,0:T(8,128)(2,1)} %all-gather.24.cloned.1.call-done, f32[512,2048]{1,0:T(8,128)} %fusion.17, bf16[512,2048]{1,0:T(8,128)(2,1)S(1)} %copy-done.2, bf16[2048,2048]{1,0:T(8,128)(2,1)} %all-gather.22.cloned.1.call-done), kind=kOutput, calls=%fused_computation.9 | convolution fusion | flops 8597274624 | bytes 25165824 | tf_op jit(solution)/shard_map/dot_general | solution.py:84
  685.7 8.0 %reduce-scatter.5.cloned.1.call-done = bf16[256,2048]{1,0:T(8,128)(2,1)} async-done(((bf16[512,2048]{1,0:T(8,128)(2,1)}), bf16[256,2048]{1,0:T(8,128)(2,1)}) %reduce-scatter.5.cloned.1.call-update) | async-done | bytes 1048592 | tf_op jit(solution)/shard_map/reduce_scatter | solution.py:83
  693.7 2.6 fusion.6
  696.3 12.0 %all-gather.26.cloned.1.call-done = bf16[512,2048]{1,0:T(8,128)(2,1)} async-done(((bf16[256,2048]{1,0:T(8,128)(2,1)}), bf16[512,2048]{1,0:T(8,128)(2,1)}) %all-gather.26.cloned.1.call-update) | async-done | bytes 2097168 | tf_op jit(solution)/shard_map/all_gather | solution.py:90
  708.3 3.2 copy.13
  (24 shorter events, 0.5 us)
Async XLA Ops:
  6.5 65.8 %copy-start = (bf16[512,2048]{1,0:T(8,128)(2,1)S(1)}, bf16[512,2048]{1,0:T(8,128)(2,1)}, u32[]{:S(2)}) copy-start(bf16[512,2048]{1,0:T(8,128)(2,1)} %param.11) | copy-start | bytes 6291460
  6.5 65.8 %all-gather.14.cloned.1.call-start = ((), (), s32[]{:S(2)}) async-start(), calls=%async_computation.4 | async-start | bytes 3538944 | tf_op jit(solution)/shard_map/all_gather | solution.py:51
  7.3 125.9 %all-gather.12.cloned.1.call-start = ((), (), s32[]{:S(2)}) async-start(), calls=%async_computation.3 | async-start | bytes 3538944 | tf_op jit(solution)/shard_map/all_gather | solution.py:53
  8.0 186.1 %all-gather.10.cloned.1.call-start = ((), (), s32[]{:S(2)}) async-start(), calls=%async_computation.2 | async-start | bytes 3538944 | tf_op jit(solution)/shard_map/all_gather | solution.py:52
  8.7 248.6 %all-gather.16.cloned.1.call-start = ((), (), s32[]{:S(2)}) async-start(), calls=%async_computation.5 | async-start | bytes 3538944 | tf_op jit(solution)/shard_map/all_gather | solution.py:54
  9.3 266.0 %reduce-scatter.3.cloned.1.call-start = ((), (), s32[]{:S(2)}) async-start(), calls=%async_computation.6 | async-start | bytes 3145728 | tf_op jit(solution)/shard_map/reduce_scatter | solution.py:70
  267.2 0.7 copy-start.1
  267.2 23.2 %all-gather.18.cloned.1.call-start = ((), (), s32[]{:S(2)}) async-start(), calls=%async_computation.7 | async-start | bytes 3145728 | tf_op jit(solution)/shard_map/all_gather | solution.py:78
  278.3 139.8 %all-gather.20.cloned.1.call-start = ((), (), s32[]{:S(2)}) async-start(), calls=%async_computation.8 | async-start | bytes 9437184 | tf_op jit(solution)/shard_map/all_gather | solution.py:55
  279.1 263.9 %all-gather.22.cloned.1.call-start = ((), (), s32[]{:S(2)}) async-start(), calls=%async_computation.9 | async-start | bytes 9437184 | tf_op jit(solution)/shard_map/all_gather | solution.py:56
  279.8 388.3 %all-gather.24.cloned.1.call-start = ((), (), s32[]{:S(2)}) async-start(), calls=%async_computation.10 | async-start | bytes 9437184 | tf_op jit(solution)/shard_map/all_gather | solution.py:57
  280.6 413.1 %reduce-scatter.5.cloned.1.call-start = ((), (), s32[]{:S(2)}) async-start(), calls=%async_computation.11 | async-start | bytes 3145728 | tf_op jit(solution)/shard_map/reduce_scatter | solution.py:83
  290.4 377.8 %copy-start.2 = (bf16[512,2048]{1,0:T(8,128)(2,1)S(1)}, bf16[512,2048]{1,0:T(8,128)(2,1)}, u32[]{:S(2)}) copy-start(bf16[512,2048]{1,0:T(8,128)(2,1)} %all-gather.18.cloned.1.call-done) | copy-start | bytes 6291460
  685.6 22.7 %all-gather.26.cloned.1.call-start = ((), (), s32[]{:S(2)}) async-start(), calls=%async_computation.12 | async-start | bytes 3145728 | tf_op jit(solution)/shard_map/all_gather | solution.py:90
Sparse Core Ops, SparseCore 0:
  9.5 62.7 all-gather.13
  74.5 58.6 all-gather.11
  135.4 58.6 all-gather.9
  196.0 61.3 all-gather.15
  267.3 7.9 reduce-scatter.2
  278.5 11.8 all-gather.17
  292.5 125.6 all-gather.19
  420.3 122.6 all-gather.21
  545.0 123.1 all-gather.23
  685.7 7.9 reduce-scatter.4
  696.4 11.8 all-gather.25
where the time goes:
time: 718 us
  waiting for transfers between devices  645 us (90%)
  matrix products  46.3 us (6%)
  between operations  13.3 us (2%)
  other arithmetic  9.09 us (1%)
    all_gather x1, waiting for transfers between devices, local(): lax.all_gather(gate_weight, 'fs', axis=0, tiled=True)  128 us
    all_gather x1, waiting for transfers between devices, local(): lax.all_gather(down_weight, 'fs', axis=1, tiled=True)  125 us
    all_gather x1, waiting for transfers between devices, local(): lax.all_gather(up_weight, 'fs', axis=0, tiled=True)  114 us
    all_gather x1, waiting for transfers between devices, local(): lax.all_gather(mix_out_weight, 'fs', axis=1, tiled=True)  63.2 us
    all_gather x1, waiting for transfers between devices, local(): lax.all_gather(value_weight, 'fs', axis=0, tiled=True)  59.4 us
    all_gather x1, waiting for transfers between devices, local(): lax.all_gather(inner_gate_weight, 'fs', axis=0, tiled=True)  57.2 us
    all_gather x1, waiting for transfers between devices, local(): lax.all_gather(outer_gate_weight, 'fs', axis=0, tiled=True)  56 us
    dot_general x1, matrix products, local(): jnp.dot(picked, down_full, preferred_element_type=jnp.float32)  17.4 us
  transfers between devices with their start and end apart: 11, of which 11 were waited for; matrix products, arithmetic and copies ran while one was open for 3% of the time, Pallas kernels for 0%

commit v1 on v0

--- a/solution.py
+++ b/solution.py
@@ -1,3 +1,4 @@
+import functools
 import jax
 import jax.numpy as jnp
 from jax import lax
@@ -5,6 +6,30 @@
 
 SEQ_GRP = 2
 EPS = 1e-05
+
+
+def kinds_wrap(local_block, axis_no):
+    carry = list(local_block.shape[1:])
+    carry[axis_no] *= local_block.shape[0]
+    kept_arr = jnp.moveaxis(local_block, 0, axis_no).reshape(carry)
+    return kept_arr
+
+
+def render_the_groups(point, link_axis, array_axis):
+    fan = lax.axis_size(link_axis)
+    ledger = [(p, (p + 1) % fan) for p in range(fan)]
+    pages = [point]
+    while len(pages) < fan:
+        extra = lax.ppermute(pages[-1], link_axis, ledger)
+        pages.append(extra)
+    reply = lax.axis_index(link_axis)
+    m_next = jnp.stack(pages, 0)
+    pages = m_next[(reply - jnp.arange(fan)) % fan]
+    mid_arr = kinds_wrap(pages, array_axis)
+    return mid_arr
+
+
+answer_groups_on = functools.partial(render_the_groups, link_axis="fs", array_axis=1)
 
 
 def rms_norm(values, gain):
@@ -51,7 +76,7 @@
         lax.all_gather(value_weight, "fs", axis=0, tiled=True),
         lax.all_gather(outer_gate_weight, "fs", axis=0, tiled=True),
         lax.all_gather(inner_gate_weight, "fs", axis=0, tiled=True),
-        lax.all_gather(mix_out_weight, "fs", axis=1, tiled=True),
+        answer_groups_on(mix_out_weight),
         lax.all_gather(gate_weight, "fs", axis=0, tiled=True),
         lax.all_gather(up_weight, "fs", axis=0, tiled=True),
         lax.all_gather(down_weight, "fs", axis=1, tiled=True),

time: 718 us -> 689 us (0.960)
  waiting for transfers between devices: 645 us -> 601 us
  local copies, waits for them, and re-layouts: 3.81 us -> 14.9 us
    ppermute x0 -> x7, waiting for transfers between devices: none -> 114 us  [render_the_groups(): extra = lax.ppermute(pages[-1], link_axis, ledger)]
    all_gather x1 -> x0, waiting for transfers between devices: 63.2 us -> none  [local(): lax.all_gather(mix_out_weight, 'fs', axis=1, tiled=True)]
    all_gather x1, waiting for transfers between devices: 59.4 us -> 0.01 us  [local(): lax.all_gather(value_weight, 'fs', axis=0, tiled=True)]
    all_gather x1, waiting for transfers between devices: 57.2 us -> 22.4 us  [local(): lax.all_gather(inner_gate_weight, 'fs', axis=0, tiled=True)]
  transfers between devices with their start and end apart: 11 -> 17, of which waited for: 11 -> 16; matrix products, arithmetic and copies ran while one was open for 3% -> 5% of each run, Pallas kernels for 0% -> 0%
where the time goes in v1:
time: 689 us
  waiting for transfers between devices  601 us (87%)
  matrix products  47.3 us (7%)
  local copies, waits for them, and re-layouts  14.9 us (2%)
  between operations  13.6 us (2%)
  other arithmetic  7.73 us (1%)
    all_gather x1, waiting for transfers between devices, local(): lax.all_gather(gate_weight, 'fs', axis=0, tiled=True)  128 us
    all_gather x1, waiting for transfers between devices, local(): lax.all_gather(down_weight, 'fs', axis=1, tiled=True)  125 us
    all_gather x1, waiting for transfers between devices, local(): lax.all_gather(up_weight, 'fs', axis=0, tiled=True)  114 us
    ppermute x7, waiting for transfers between devices, render_the_groups(): extra = lax.ppermute(pages[-1], link_axis, ledger)  114 us
    all_gather x1, waiting for transfers between devices, local(): lax.all_gather(outer_gate_weight, 'fs', axis=0, tiled=True)  56 us
    all_gather x1, waiting for transfers between devices, local(): lax.all_gather(inner_gate_weight, 'fs', axis=0, tiled=True)  22.4 us
    dot_general x1, matrix products, local(): jnp.dot(picked, down_full, preferred_element_type=jnp.float32)  17.4 us
  transfers between devices with their start and end apart: 17, of which 16 were waited for; matrix products, arithmetic and copies ran while one was open for 5% of the time, Pallas kernels for 0%

profile of v1, /device:TPU:0, one launch (start us, length us, event | category | flops | bytes accessed | tf_op | source)
XLA Modules:
  0.0 688.6 jit_solution(9808848247303414814)
XLA Ops:
  8.8 3.0 collective-permute-start
  11.8 12.5 %collective-permute-done = bf16[768,256]{1,0:T(8,128)(2,1)S(1)} collective-permute-done((bf16[768,256]{1,0:T(8,128)(2,1)}, bf16[768,256]{1,0:T(8,128)(2,1)S(1)}, u32[]{:S(2)}, u32[]{:S(2)}) %collective-permute-start) | collective-permute-done | bytes 393248 | tf_op jit(solution)/shard_map/ppermute | solution.py:23
  24.3 2.1 fusion
  26.4 20.4 %collective-permute-done.1 = bf16[768,256]{1,0:T(8,128)(2,1)S(1)} collective-permute-done((bf16[768,256]{1,0:T(8,128)(2,1)S(1)}, bf16[768,256]{1,0:T(8,128)(2,1)S(1)}, u32[]{:S(2)}, u32[]{:S(2)}) %collective-permute-start.1) | collective-permute-done | bytes 393248 | tf_op jit(solution)/shard_map/ppermute | solution.py:23
  46.8 19.6 %collective-permute-done.2 = bf16[768,256]{1,0:T(8,128)(2,1)S(1)} collective-permute-done((bf16[768,256]{1,0:T(8,128)(2,1)S(1)}, bf16[768,256]{1,0:T(8,128)(2,1)S(1)}, u32[]{:S(2)}, u32[]{:S(2)}) %collective-permute-start.2) | collective-permute-done | bytes 393248 | tf_op jit(solution)/shard_map/ppermute | solution.py:23
  66.5 0.8 bitcast_dynamic-update-slice_fusion.7
  67.3 20.4 %collective-permute-done.3 = bf16[768,256]{1,0:T(8,128)(2,1)S(1)} collective-permute-done((bf16[768,256]{1,0:T(8,128)(2,1)S(1)}, bf16[768,256]{1,0:T(8,128)(2,1)S(1)}, u32[]{:S(2)}, u32[]{:S(2)}) %collective-permute-start.3) | collective-permute-done | bytes 393248 | tf_op jit(solution)/shard_map/ppermute | solution.py:23
  88.5 0.8 bitcast_dynamic-update-slice_fusion.5
  89.3 12.0 %collective-permute-done.4 = bf16[768,256]{1,0:T(8,128)(2,1)S(1)} collective-permute-done((bf16[768,256]{1,0:T(8,128)(2,1)S(1)}, bf16[768,256]{1,0:T(8,128)(2,1)S(1)}, u32[]{:S(2)}, u32[]{:S(2)}) %collective-permute-start.4) | collective-permute-done | bytes 393248 | tf_op jit(solution)/shard_map/ppermute | solution.py:23
  102.8 10.0 %collective-permute-done.5 = bf16[768,256]{1,0:T(8,128)(2,1)S(1)} collective-permute-done((bf16[768,256]{1,0:T(8,128)(2,1)S(1)}, bf16[768,256]{1,0:T(8,128)(2,1)S(1)}, u32[]{:S(2)}, u32[]{:S(2)}) %collective-permute-start.5) | collective-permute-done | bytes 393248 | tf_op jit(solution)/shard_map/ppermute | solution.py:23
  114.4 18.8 %collective-permute-done.6 = bf16[768,256]{1,0:T(8,128)(2,1)S(1)} collective-permute-done((bf16[768,256]{1,0:T(8,128)(2,1)S(1)}, bf16[768,256]{1,0:T(8,128)(2,1)S(1)}, u32[]{:S(2)}, u32[]{:S(2)}) %collective-permute-start.6) | collective-permute-done | bytes 393248 | tf_op jit(solution)/shard_map/ppermute | solution.py:23
  133.1 0.8 bitcast_dynamic-update-slice_fusion
  133.9 2.6 gather_fusion
  136.5 2.8 copy.12
  139.3 4.5 convolution_convert_fusion.2
  143.9 22.4 %all-gather.11.cloned.1.call-done = bf16[2048,768]{1,0:T(8,128)(2,1)} async-done(((bf16[256,768]{1,0:T(8,128)(2,1)}), bf16[2048,768]{1,0:T(8,128)(2,1)}) %all-gather.11.cloned.1.call-update) | async-done | bytes 3145744 | tf_op jit(solution)/shard_map/all_gather | solution.py:78
  166.3 4.9 convert_multiply_fusion.4
  171.2 56.0 %all-gather.9.cloned.1.call-done = bf16[2048,768]{1,0:T(8,128)(2,1)} async-done(((bf16[256,768]{1,0:T(8,128)(2,1)}), bf16[2048,768]{1,0:T(8,128)(2,1)}) %all-gather.9.cloned.1.call-update) | async-done | bytes 3145744 | tf_op jit(solution)/shard_map/all_gather | solution.py:77
  227.2 9.9 %convolution_convert_fusion.1 = bf16[512,2048]{1,0:T(8,128)(2,1)} fusion(bf16[768,2048]{0,1:T(8,128)(2,1)} %bitcast.41, f32[512,768]{1,0:T(8,128)} %convert_multiply_fusion.4, f32[511,768]{1,0:T(8,128)} %bitcast.42, f32[510,768]{1,0:T(8,128)} %bitcast.43, bf16[2048,768]{1,0:T(8,128)(2,1)} %all-gather.9.cloned.1.call-done, f32[768]{0:T(1024)S(1)} %get-tuple-element.6, ...), kind=kOutput, calls=%fused_computation.11 | convolution fusion | flops 3230793728 | bytes 15215616 | tf_op jit(solution)/shard_map/dot_general | solution.py:96
  237.2 8.5 %reduce-scatter.3.cloned.1.call-done = bf16[256,2048]{1,0:T(8,128)(2,1)} async-done(((bf16[512,2048]{1,0:T(8,128)(2,1)}), bf16[256,2048]{1,0:T(8,128)(2,1)}) %reduce-scatter.3.cloned.1.call-update) | async-done | bytes 1048592 | tf_op jit(solution)/shard_map/reduce_scatter | solution.py:95
  245.7 1.7 fusion.3
  247.5 1.3 fusion.5
  251.1 9.7 %all-gather.15.cloned.1.call-done = bf16[512,2048]{1,0:T(8,128)(2,1)} async-done(((bf16[256,2048]{1,0:T(8,128)(2,1)}), bf16[512,2048]{1,0:T(8,128)(2,1)}) %all-gather.15.cloned.1.call-update) | async-done | bytes 2097168 | tf_op jit(solution)/shard_map/all_gather | solution.py:103
  260.8 127.7 %all-gather.17.cloned.1.call-done = bf16[2048,2048]{1,0:T(8,128)(2,1)} async-done(((bf16[256,2048]{1,0:T(8,128)(2,1)}), bf16[2048,2048]{1,0:T(8,128)(2,1)}) %all-gather.17.cloned.1.call-update) | async-done | bytes 8388624 | tf_op jit(solution)/shard_map/all_gather | solution.py:80
  388.5 10.5 %fusion.19 = f32[512,2048]{1,0:T(8,128)} fusion(bf16[512,2048]{1,0:T(8,128)(2,1)} %all-gather.15.cloned.1.call-done, bf16[2048,2048]{1,0:T(8,128)(2,1)} %all-gather.17.cloned.1.call-done), kind=kOutput, calls=%fused_computation.50 | convolution fusion | flops 4294967296 | bytes 14680064 | tf_op jit(solution)/shard_map/dot_general | solution.py:104
  399.0 114.3 %all-gather.19.cloned.1.call-done = bf16[2048,2048]{1,0:T(8,128)(2,1)} async-done(((bf16[256,2048]{1,0:T(8,128)(2,1)}), bf16[2048,2048]{1,0:T(8,128)(2,1)}) %all-gather.19.cloned.1.call-update) | async-done | bytes 8388624 | tf_op jit(solution)/shard_map/all_gather | solution.py:81
  513.3 125.2 %all-gather.21.cloned.1.call-done = bf16[2048,2048]{1,0:T(8,128)(2,1)} async-done(((bf16[2048,256]{1,0:T(8,128)(2,1)}), bf16[2048,2048]{1,0:T(8,128)(2,1)}) %all-gather.21.cloned.1.call-update) | async-done | bytes 8388624 | tf_op jit(solution)/shard_map/all_gather | solution.py:82
  638.5 17.4 %convolution_convert_fusion = bf16[512,2048]{1,0:T(8,128)(2,1)} fusion(bf16[2048,2048]{1,0:T(8,128)(2,1)} %all-gather.21.cloned.1.call-done, f32[512,2048]{1,0:T(8,128)} %fusion.19, bf16[512,2048]{1,0:T(8,128)(2,1)S(1)} %copy-done.5, bf16[2048,2048]{1,0:T(8,128)(2,1)} %all-gather.19.cloned.1.call-done), kind=kOutput, calls=%fused_computation.10 | convolution fusion | flops 8597274624 | bytes 25165824 | tf_op jit(solution)/shard_map/dot_general | solution.py:109
  656.0 8.0 %reduce-scatter.5.cloned.1.call-done = bf16[256,2048]{1,0:T(8,128)(2,1)} async-done(((bf16[512,2048]{1,0:T(8,128)(2,1)}), bf16[256,2048]{1,0:T(8,128)(2,1)}) %reduce-scatter.5.cloned.1.call-update) | async-done | bytes 1048592 | tf_op jit(solution)/shard_map/reduce_scatter | solution.py:108
  664.0 2.6 fusion.6
  666.6 12.0 %all-gather.23.cloned.1.call-done = bf16[512,2048]{1,0:T(8,128)(2,1)} async-done(((bf16[256,2048]{1,0:T(8,128)(2,1)}), bf16[512,2048]{1,0:T(8,128)(2,1)}) %all-gather.23.cloned.1.call-update) | async-done | bytes 2097168 | tf_op jit(solution)/shard_map/all_gather | solution.py:115
  678.6 3.2 copy.21
  (53 shorter events, 8.6 us)
Async XLA Ops:
  6.5 59.9 %copy-start.1 = (bf16[768,256]{1,0:T(8,128)(2,1)S(1)}, bf16[768,256]{1,0:T(8,128)(2,1)}, u32[]{:S(2)}) copy-start(bf16[768,256]{1,0:T(8,128)(2,1)} %param.17) | copy-start | bytes 1179652
  6.5 59.9 %copy-start.3 = (bf16[2048]{0:T(1024)(128)(2,1)S(1)}, bf16[2048]{0:T(1024)(128)(2,1)}, u32[]{:S(2)}) copy-start(bf16[2048]{0:T(1024)(128)(2,1)} %param.12) | copy-start | bytes 12292
  6.5 59.9 %copy-start.2 = (bf16[3,768]{1,0:T(4,128)(2,1)S(1)}, bf16[3,768]{1,0:T(4,128)(2,1)}, u32[]{:S(2)}) copy-start(bf16[3,768]{1,0:T(4,128)(2,1)} %param.16) | copy-start | bytes 13828
  6.5 132.8 %all-gather.13.cloned.1.call-start = ((), (), s32[]{:S(2)}) async-start(), calls=%async_computation.4 | async-start | bytes 3538944 | tf_op jit(solution)/shard_map/all_gather | solution.py:76
  7.3 159.0 %all-gather.11.cloned.1.call-start = ((), (), s32[]{:S(2)}) async-start(), calls=%async_computation.3 | async-start | bytes 3538944 | tf_op jit(solution)/shard_map/all_gather | solution.py:78
  8.0 219.2 %all-gather.9.cloned.1.call-start = ((), (), s32[]{:S(2)}) async-start(), calls=%async_computation.2 | async-start | bytes 3538944 | tf_op jit(solution)/shard_map/all_gather | solution.py:77
  8.7 237.0 %reduce-scatter.3.cloned.1.call-start = ((), (), s32[]{:S(2)}) async-start(), calls=%async_computation.5 | async-start | bytes 3145728 | tf_op jit(solution)/shard_map/reduce_scatter | solution.py:95
  8.8 15.5 %collective-permute-start = (bf16[768,256]{1,0:T(8,128)(2,1)}, bf16[768,256]{1,0:T(8,128)(2,1)S(1)}, u32[]{:S(2)}, u32[]{:S(2)}) collective-permute-start(bf16[768,256]{1,0:T(8,128)(2,1)} %param.17), channel_id=1, source_target_pairs={{0,2},{2,4},{4,6},{6,8},{8,10},{10,12},{12,14},{14,0},{1,3},{3,5},... | collective-permute-start | bytes 1179656 | tf_op jit(solution)/shard_map/ppermute | solution.py:23
  24.3 22.5 %collective-permute-start.1 = (bf16[768,256]{1,0:T(8,128)(2,1)S(1)}, bf16[768,256]{1,0:T(8,128)(2,1)S(1)}, u32[]{:S(2)}, u32[]{:S(2)}) collective-permute-start(bf16[768,256]{1,0:T(8,128)(2,1)S(1)} %collective-permute-done), channel_id=1, source_target_pairs={{0,2},{2,4},{4,6},{6,8},{8,10},{10,12},{12,14},{14,0},{1,3},{3,5},... | collective-permute-start | bytes 1179656 | tf_op jit(solution)/shard_map/ppermute | solution.py:23
  46.8 19.6 %collective-permute-start.2 = (bf16[768,256]{1,0:T(8,128)(2,1)S(1)}, bf16[768,256]{1,0:T(8,128)(2,1)S(1)}, u32[]{:S(2)}, u32[]{:S(2)}) collective-permute-start(bf16[768,256]{1,0:T(8,128)(2,1)S(1)} %collective-permute-done.1), channel_id=1, source_target_pairs={{0,2},{2,4},{4,6},{6,8},{8,10},{10,12},{12,14},{14,0},{1,3},{3,5},... | collective-permute-start | bytes 1179656 | tf_op jit(solution)/shard_map/ppermute | solution.py:23
  66.4 21.3 %collective-permute-start.3 = (bf16[768,256]{1,0:T(8,128)(2,1)S(1)}, bf16[768,256]{1,0:T(8,128)(2,1)S(1)}, u32[]{:S(2)}, u32[]{:S(2)}) collective-permute-start(bf16[768,256]{1,0:T(8,128)(2,1)S(1)} %collective-permute-done.2), channel_id=1, source_target_pairs={{0,2},{2,4},{4,6},{6,8},{8,10},{10,12},{12,14},{14,0},{1,3},{3,5},... | collective-permute-start | bytes 1179656 | tf_op jit(solution)/shard_map/ppermute | solution.py:23
  87.7 13.5 %collective-permute-start.4 = (bf16[768,256]{1,0:T(8,128)(2,1)S(1)}, bf16[768,256]{1,0:T(8,128)(2,1)S(1)}, u32[]{:S(2)}, u32[]{:S(2)}) collective-permute-start(bf16[768,256]{1,0:T(8,128)(2,1)S(1)} %collective-permute-done.3), channel_id=1, source_target_pairs={{0,2},{2,4},{4,6},{6,8},{8,10},{10,12},{12,14},{14,0},{1,3},{3,5},... | collective-permute-start | bytes 1179656 | tf_op jit(solution)/shard_map/ppermute | solution.py:23
  101.2 11.6 %collective-permute-start.5 = (bf16[768,256]{1,0:T(8,128)(2,1)S(1)}, bf16[768,256]{1,0:T(8,128)(2,1)S(1)}, u32[]{:S(2)}, u32[]{:S(2)}) collective-permute-start(bf16[768,256]{1,0:T(8,128)(2,1)S(1)} %collective-permute-done.4), channel_id=1, source_target_pairs={{0,2},{2,4},{4,6},{6,8},{8,10},{10,12},{12,14},{14,0},{1,3},{3,5},... | collective-permute-start | bytes 1179656 | tf_op jit(solution)/shard_map/ppermute | solution.py:23
  112.8 20.3 %collective-permute-start.6 = (bf16[768,256]{1,0:T(8,128)(2,1)S(1)}, bf16[768,256]{1,0:T(8,128)(2,1)S(1)}, u32[]{:S(2)}, u32[]{:S(2)}) collective-permute-start(bf16[768,256]{1,0:T(8,128)(2,1)S(1)} %collective-permute-done.5), channel_id=1, source_target_pairs={{0,2},{2,4},{4,6},{6,8},{8,10},{10,12},{12,14},{14,0},{1,3},{3,5},... | collective-permute-start | bytes 1179656 | tf_op jit(solution)/shard_map/ppermute | solution.py:23
  139.3 27.0 %copy-start = (bf16[512,2048]{1,0:T(8,128)(2,1)S(1)}, bf16[512,2048]{1,0:T(8,128)(2,1)}, u32[]{:S(2)}) copy-start(bf16[512,2048]{1,0:T(8,128)(2,1)} %param.11) | copy-start | bytes 6291460
  227.2 10.0 %copy-start.4 = (bf16[2048]{0:T(1024)(128)(2,1)S(1)}, bf16[2048]{0:T(1024)(128)(2,1)}, u32[]{:S(2)}) copy-start(bf16[2048]{0:T(1024)(128)(2,1)} %param.18) | copy-start | bytes 12292
  237.2 23.6 %all-gather.15.cloned.1.call-start = ((), (), s32[]{:S(2)}) async-start(), calls=%async_computation.6 | async-start | bytes 3145728 | tf_op jit(solution)/shard_map/all_gather | solution.py:103
  248.8 139.7 %all-gather.17.cloned.1.call-start = ((), (), s32[]{:S(2)}) async-start(), calls=%async_computation.7 | async-start | bytes 9437184 | tf_op jit(solution)/shard_map/all_gather | solution.py:80
  249.4 263.9 %all-gather.19.cloned.1.call-start = ((), (), s32[]{:S(2)}) async-start(), calls=%async_computation.8 | async-start | bytes 9437184 | tf_op jit(solution)/shard_map/all_gather | solution.py:81
  250.1 388.3 %all-gather.21.cloned.1.call-start = ((), (), s32[]{:S(2)}) async-start(), calls=%async_computation.9 | async-start | bytes 9437184 | tf_op jit(solution)/shard_map/all_gather | solution.py:82
  250.9 413.1 %reduce-scatter.5.cloned.1.call-start = ((), (), s32[]{:S(2)}) async-start(), calls=%async_computation.10 | async-start | bytes 3145728 | tf_op jit(solution)/shard_map/reduce_scatter | solution.py:108
  260.8 377.7 %copy-start.5 = (bf16[512,2048]{1,0:T(8,128)(2,1)S(1)}, bf16[512,2048]{1,0:T(8,128)(2,1)}, u32[]{:S(2)}) copy-start(bf16[512,2048]{1,0:T(8,128)(2,1)} %all-gather.15.cloned.1.call-done) | copy-start | bytes 6291460
  655.9 22.7 %all-gather.23.cloned.1.call-start = ((), (), s32[]{:S(2)}) async-start(), calls=%async_computation.11 | async-start | bytes 3145728 | tf_op jit(solution)/shard_map/all_gather | solution.py:115
Sparse Core Ops, SparseCore 0:
  9.5 82.8 all-gather.12
  94.6 71.6 all-gather.10
  168.5 58.6 all-gather.8
  237.3 8.4 reduce-scatter.2
  248.9 11.8 all-gather.14
  262.8 125.6 all-gather.16
  390.6 122.6 all-gather.18
  515.3 123.1 all-gather.20
  656.0 7.8 reduce-scatter.4
  666.7 11.8 all-gather.22
